TPU v7x, 32 devices: a whole 2x2x4 slice. The times are simulated.
32 devices in a mesh: grp: 2 (over y), fs: 4 (over z), tp: 4 (over x, core).
Axes of the slice: x: 2, y: 2, z: 4, core: 2. Of those that a mesh axis runs over, the one named last changes fastest.
Arguments:
- tokens: bfloat16 [512, 2048], P(('grp', 'fs')), parts along dimension 0, may hold values from -6 to 6
- routes: int32 [512, 2], P(('grp', 'fs')), parts along dimension 0, may hold values from 0 to 3, as said below
- route_logits: float32 [512, 2], P(('grp', 'fs')), parts along dimension 0, may hold values from -8 to 8
- gain: float32 [2048], P('fs'), may hold values from 0.1 to 1.9
- w_gate: float32 [4, 2048, 7168], P(None, 'fs', 'tp'), may hold values from -0.125 to 0.125
- w_up: float32 [4, 2048, 7168], P(None, 'fs', 'tp'), may hold values from -0.125 to 0.125
- w_down: float32 [4, 7168, 2048], P(None, 'fs', 'tp'), may hold values from -0.0625 to 0.0625
Outputs:
- gate_served: bfloat16 [8, 2048, 7168], P(('grp', 'tp'), None, 'fs'), parts along dimension 0
- up_served: bfloat16 [8, 2048, 7168], P(('grp', 'tp'), None, 'fs'), parts along dimension 0
- down_served: bfloat16 [8, 7168, 2048], P(('grp', 'tp'), 'fs'), parts along dimension 0
- mixed: bfloat16 [512, 2048], P(('grp', 'fs'), 'tp'), parts along dimension 0
There are 2 independent parts, one for each index of `grp`. A program takes and returns all parts, laid end to end along the dimension named above; an argument that names none is the same for every part. Nothing has to cross between parts.
Inputs may be any that keep to these rules, and one draw needn't show every extreme that they name: `routes`: each row names 2 different experts; every expert is named by some row.
All inputs are finite; a program needn't handle non-finite values.
Results may differ from a plain program's by a relative error of at most 0.0085.
Values may be sent and summed in bfloat16 or wider, within the bound.
A program may use at most 192 MiB of HBM per device.

v0:
```python
import jax
import jax.numpy as jnp
from jax import lax
from jax.sharding import PartitionSpec as P


def body(tokens, routes, route_logits, gain, w_gate, w_up, w_down):
    gate_cast = (w_gate * gain[None, :, None]).astype(jnp.bfloat16)
    up_cast = (w_up * gain[None, :, None]).astype(jnp.bfloat16)
    down_cast = w_down.astype(jnp.bfloat16)
    gate_tp, up_tp, down_served = (
        lax.all_to_all(gate_cast, "tp", split_axis=0, concat_axis=2, tiled=True),
        lax.all_to_all(up_cast, "tp", split_axis=0, concat_axis=2, tiled=True),
        lax.all_to_all(down_cast, "tp", split_axis=0, concat_axis=2, tiled=True),
    )
    gate_served, up_served = (
        lax.all_to_all(gate_tp, "fs", split_axis=2, concat_axis=1, tiled=True),
        lax.all_to_all(up_tp, "fs", split_axis=2, concat_axis=1, tiled=True),
    )
    values = tokens.astype(jnp.float32)
    mean_square = jnp.mean(values * values, axis=-1, keepdims=True)
    normed = (values * lax.rsqrt(mean_square + 1e-06)).astype(jnp.bfloat16)
    expert_id = lax.axis_index("tp")
    first = jax.nn.sigmoid(route_logits[:, 0] - route_logits[:, 1])
    second = jax.nn.sigmoid(route_logits[:, 1] - route_logits[:, 0])
    weight_col = first * (routes[:, 0] == expert_id).astype(jnp.float32)
    weight_col = (weight_col + second * (routes[:, 1] == expert_id).astype(jnp.float32)).astype(
        jnp.bfloat16
    )
    gate_local = gate_served[0]
    up_local = up_served[0]
    piece_rows = lax.all_gather(normed, "fs", axis=0, tiled=True)
    piece_weight = lax.all_gather(weight_col, "fs", axis=0, tiled=True)
    gate_act = jnp.dot(piece_rows, gate_local, preferred_element_type=jnp.float32)
    up_act = jnp.dot(piece_rows, up_local, preferred_element_type=jnp.float32)
    hidden_rows = jax.nn.silu(gate_act) * up_act * piece_weight[:, None].astype(jnp.float32)
    hidden = hidden_rows.astype(jnp.bfloat16)
    down_local = down_served[0]
    term = jnp.dot(hidden, down_local, preferred_element_type=jnp.float32)
    by_feature = lax.psum_scatter(term, "tp", scatter_dimension=1, tiled=True)
    mixed = lax.psum_scatter(by_feature, "fs", scatter_dimension=0, tiled=True)
    return (gate_served, up_served, down_served, mixed.astype(jnp.bfloat16))


def solution(mesh):
    return jax.shard_map(
        body,
        mesh=mesh,
        in_specs=(
            P(("grp", "fs"), None),
            P(("grp", "fs"), None),
            P(("grp", "fs"), None),
            P("fs"),
            P(None, "fs", "tp"),
            P(None, "fs", "tp"),
            P(None, "fs", "tp"),
        ),
        out_specs=(
            P(("grp", "tp"), None, "fs"),
            P(("grp", "tp"), None, "fs"),
            P(("grp", "tp"), "fs", None),
            P(("grp", "fs"), "tp"),
        ),
        check_vma=False,
    )
```

profile of v0, /device:TPU:0, one launch (start us, length us, event | category | flops | bytes accessed | tf_op | source)
XLA Modules:
  0.0 715.9 jit_solution(18152583940366378702)
XLA Ops:
  7.2 14.4 %copy.24 = f32[4,512,1792]{1,2,0:T(8,128)} copy(f32[4,512,1792]{2,1,0:T(8,128)} %param.11) | data formatting | bytes 29360128 | tf_op args[4]
  21.5 14.3 %copy.27 = f32[4,512,1792]{1,2,0:T(8,128)} copy(f32[4,512,1792]{2,1,0:T(8,128)} %param.12) | data formatting | bytes 29360128 | tf_op args[5]
  35.8 13.5 %multiply_convert_fusion = (bf16[4,512,1792]{1,2,0:T(8,128)(2,1)}, bf16[4,512,1792]{1,2,0:T(8,128)(2,1)S(1)}) fusion(f32[4,512,1792]{1,2,0:T(8,128)} %copy.27, f32[512]{0:T(512)S(1)} %copy-done.1, f32[4,512,1792]{1,2,0:T(8,128)} %copy.24), kind=kLoop, calls=%fused_computation | loop fusion | flops 14680064 | bytes 44042240 | tf_op jit(solution)/shard_map/convert_element_type | solution.py:9
  49.3 86.2 %all_to_all.90 = bf16[4,512,1792]{1,2,0:T(8,128)(2,1)} all-to-all(bf16[4,512,1792]{1,2,0:T(8,128)(2,1)S(1)} %get-tuple-element.17), channel_id=1, replica_groups=mesh['grp'=2,'fs'=4,'tp'=4] {'tp'}, dimensions={0} | all-to-all | bytes 14680064 | tf_op jit(solution)/shard_map/all_to_all | solution.py:12
  135.5 5.4 all-to-all-start.2
  140.9 13.7 %copy.39 = bf16[1,512,7168]{1,0,2:T(2,128)(2,1)} copy(bf16[1,512,7168]{1,2,0:T(8,128)(2,1)} %bitcast.47) | data formatting | bytes 14680064 | tf_op jit(solution)/shard_map/all_to_all | solution.py:12
  155.2 48.2 %reduce = bf16[7168,512]{1,0:T(8,128)(2,1)} reduce(bf16[7168,1,512]{2,1,0:T(2,128)(2,1)} %bitcast.43, bf16[]{:T(256)} %broadcast.43), dimensions={1}, to_apply=%bitcast.42.reduce_sub_computation | reduce | bytes 14680066
  203.4 9.0 %reshape.55 = bf16[4,2,458752]{2,1,0:T(2,128)(2,1)} reshape(bf16[7168,512]{1,0:T(8,128)(2,1)} %reduce) | data formatting | bytes 14680064
  212.4 10.5 %all-to-all-done.2 = bf16[4,512,1792]{1,2,0:T(8,128)(2,1)} async-done(((bf16[4,512,1792]{1,2,0:T(8,128)(2,1)}), bf16[4,512,1792]{1,2,0:T(8,128)(2,1)}, u32[]{:S(2)}, u32[]{:S(2)}) %all-to-all-start.2) | async-done | bytes 7340064 | tf_op jit(solution)/shard_map/all_to_all | solution.py:13
  222.8 5.7 all-to-all-start.1
  228.5 13.7 %copy.38 = bf16[1,512,7168]{1,0,2:T(2,128)(2,1)} copy(bf16[1,512,7168]{1,2,0:T(8,128)(2,1)} %bitcast.7) | data formatting | bytes 14680064 | tf_op jit(solution)/shard_map/all_to_all | solution.py:13
  242.2 48.2 %reduce.1 = bf16[7168,512]{1,0:T(8,128)(2,1)} reduce(bf16[7168,1,512]{2,1,0:T(2,128)(2,1)} %bitcast.44, bf16[]{:T(256)} %broadcast.43), dimensions={1}, to_apply=%bitcast.41.reduce_sub_computation | reduce | bytes 14680066
  290.4 9.0 %reshape.57 = bf16[4,2,458752]{2,1,0:T(2,128)(2,1)} reshape(bf16[7168,512]{1,0:T(8,128)(2,1)} %reduce.1) | data formatting | bytes 14680064
  299.4 90.4 %all-to-all-done.1 = bf16[4,2,458752]{2,1,0:T(2,128)(2,1)} async-done(((bf16[4,2,458752]{2,1,0:T(2,128)(2,1)}), bf16[4,2,458752]{2,1,0:T(2,128)(2,1)}, u32[]{:S(2)}, u32[]{:S(2)}) %all-to-all-start.1) | async-done | bytes 7340064 | tf_op jit(solution)/shard_map/all_to_all | solution.py:17
  389.8 5.5 all-to-all-start.3
  395.3 11.6 %copy.30 = bf16[4,1792,512]{1,2,0:T(8,128)(2,1)} copy(f32[4,1792,512]{2,1,0:T(8,128)} %param.13) | data formatting | bytes 22020096 | tf_op args[6]
  407.0 148.5 %all-to-all-done.3 = bf16[4,2,458752]{2,1,0:T(2,128)(2,1)} async-done(((bf16[4,2,458752]{2,1,0:T(2,128)(2,1)}), bf16[4,2,458752]{2,1,0:T(2,128)(2,1)}, u32[]{:S(2)}, u32[]{:S(2)}) %all-to-all-start.3) | async-done | bytes 7340064 | tf_op jit(solution)/shard_map/all_to_all | solution.py:18
  555.4 5.4 all-to-all-start.4
  561.1 0.8 fusion.4
  563.5 10.1 %all-reduce = bf16[256]{0:T(256)(128)(2,1)S(1)} all-reduce(bf16[256]{0:T(256)(128)(2,1)S(1)} %dynamic-update-slice), channel_id=2, replica_groups=mesh['grp'=2,'fs'=4,'tp'=4] {'fs'}, use_global_device_ids=true, to_apply=%add | all-reduce | flops 256 | bytes 1024
  573.7 11.3 %reshape.56 = bf16[7168,1,512]{2,1,0:T(2,128)(2,1)} reshape(bf16[4,2,458752]{2,1,0:T(2,128)(2,1)} %all-to-all-done.1) | data formatting | bytes 14680064
  585.0 10.4 %copy.34 = bf16[1,512,7168]{1,2,0:T(8,128)(2,1)} copy(bf16[1,512,7168]{1,0,2:T(2,128)(2,1)} %bitcast.45) | data formatting | bytes 14680064
  595.4 9.9 %copy.26 = bf16[1,4,512,1792]{3,2,1,0:T(8,128)(2,1)} copy(bf16[1,4,512,1792]{2,3,1,0:T(8,128)(2,1)} %bitcast.48) | data formatting | bytes 14680064 | tf_op jit(solution)/shard_map/all_to_all | solution.py:17
  605.3 11.3 %reshape.58 = bf16[7168,1,512]{2,1,0:T(2,128)(2,1)} reshape(bf16[4,2,458752]{2,1,0:T(2,128)(2,1)} %all-to-all-done.3) | data formatting | bytes 14680064
  616.6 10.4 %copy.35 = bf16[1,512,7168]{1,2,0:T(8,128)(2,1)} copy(bf16[1,512,7168]{1,0,2:T(2,128)(2,1)} %bitcast.46) | data formatting | bytes 14680064
  627.0 9.9 %copy.29 = bf16[1,4,512,1792]{3,2,1,0:T(8,128)(2,1)} copy(bf16[1,4,512,1792]{2,3,1,0:T(8,128)(2,1)} %bitcast.49) | data formatting | bytes 14680064 | tf_op jit(solution)/shard_map/all_to_all | solution.py:18
  637.0 5.5 fusion.7
  642.8 11.1 %fusion.2 = f32[256,2048]{1,0:T(8,128)} fusion(bf16[1792,2048]{0,1:T(8,128)(2,1)} %bitcast.18, bf16[256,2048]{1,0:T(8,128)(2,1)S(1)} %copy-done.4, bf16[2048,1792]{1,0:T(8,128)(2,1)} %bitcast.52, f32[256,1792]{1,0:T(8,128)S(1)} %fusion.7, f32[256]{0:T(256)S(1)} %convert_element_type.41), kind=kOutput, calls=%fused_computation.5 | convolution fusion | flops 3761307648 | bytes 19661824 | tf_op jit(solution)/shard_map/dot_general | solution.py:39
  653.9 29.7 %reduce-scatter.3.cloned.1.call-done = f32[256,512]{1,0:T(8,128)} async-done(((f32[256,2048]{1,0:T(8,128)}), f32[256,512]{1,0:T(8,128)}) %reduce-scatter.3.cloned.1.call-update) | async-done | bytes 524304 | tf_op jit(solution)/shard_map/reduce_scatter | solution.py:40
  683.7 10.4 %copy.33 = bf16[1,1792,2048]{2,1,0:T(8,128)(2,1)} copy(bf16[1,1792,2048]{1,2,0:T(8,128)(2,1)} %bitcast.12) | data formatting | bytes 14680064
  694.1 13.7 %reduce-scatter.5.cloned.1.call-done = f32[64,512]{1,0:T(8,128)} async-done(((f32[256,512]{1,0:T(8,128)}), f32[64,512]{1,0:T(8,128)}) %reduce-scatter.5.cloned.1.call-update) | async-done | bytes 131088 | tf_op jit(solution)/shard_map/reduce_scatter | solution.py:41
  707.8 1.5 convert_element_type.38
  (28 shorter events, 2.0 us)
Async XLA Ops:
  21.5 14.3 %copy-start.1 = (f32[512]{0:T(512)S(1)}, f32[512]{0:T(512)}, u32[]{:S(2)}) copy-start(f32[512]{0:T(512)} %param.10) | copy-start | bytes 6148
  135.5 87.3 %all-to-all-start.2 = ((bf16[4,512,1792]{1,2,0:T(8,128)(2,1)}), bf16[4,512,1792]{1,2,0:T(8,128)(2,1)}, u32[]{:S(2)}, u32[]{:S(2)}) async-start(bf16[4,512,1792]{1,2,0:T(8,128)(2,1)} %get-tuple-element.16), calls=%async_computation.2 | async-start | bytes 14680064 | tf_op jit(solution)/shard_map/all_to_all | solution.py:13
  222.8 167.0 %all-to-all-start.1 = ((bf16[4,2,458752]{2,1,0:T(2,128)(2,1)}), bf16[4,2,458752]{2,1,0:T(2,128)(2,1)}, u32[]{:S(2)}, u32[]{:S(2)}) async-start(bf16[4,2,458752]{2,1,0:T(2,128)(2,1)} %reshape.55), calls=%async_computation.1 | async-start | bytes 14680064 | tf_op jit(solution)/shard_map/all_to_all | solution.py:17
  389.8 165.6 %all-to-all-start.3 = ((bf16[4,2,458752]{2,1,0:T(2,128)(2,1)}), bf16[4,2,458752]{2,1,0:T(2,128)(2,1)}, u32[]{:S(2)}, u32[]{:S(2)}) async-start(bf16[4,2,458752]{2,1,0:T(2,128)(2,1)} %reshape.57), calls=%async_computation.3 | async-start | bytes 14680064 | tf_op jit(solution)/shard_map/all_to_all | solution.py:18
  407.0 154.0 %copy-start = (bf16[64,2048]{1,0:T(8,128)(2,1)S(1)}, bf16[64,2048]{1,0:T(8,128)(2,1)}, u32[]{:S(2)}) copy-start(bf16[64,2048]{1,0:T(8,128)(2,1)} %param.7) | copy-start | bytes 786436
  407.0 155.0 %copy-start.5 = (u32[32]{0:T(128)S(1)}, u32[32]{0:T(128)}, u32[]{:S(2)}) copy-start(u32[32]{0:T(128)} %constant.19) | copy-start | bytes 388
  407.0 156.3 %copy-start.2 = (s32[64,2]{0,1:T(2,128)S(1)}, s32[64,2]{0,1:T(2,128)}, u32[]{:S(2)}) copy-start(s32[64,2]{0,1:T(2,128)} %param.8) | copy-start | bytes 1540
  407.0 156.3 %copy-start.3 = (f32[64,2]{0,1:T(2,128)S(1)}, f32[64,2]{0,1:T(2,128)}, u32[]{:S(2)}) copy-start(f32[64,2]{0,1:T(2,128)} %param.9) | copy-start | bytes 1540
  555.4 87.3 %all-to-all-start.4 = ((bf16[4,1792,512]{1,2,0:T(8,128)(2,1)}), bf16[4,1792,512]{1,2,0:T(8,128)(2,1)}, u32[]{:S(2)}, u32[]{:S(2)}) async-start(bf16[4,1792,512]{1,2,0:T(8,128)(2,1)} %copy.30), calls=%async_computation.4 | async-start | bytes 14680064 | tf_op jit(solution)/shard_map/all_to_all | solution.py:14
  560.9 76.1 %all-gather.3.cloned.1.call-start = ((), (), s32[]{:S(2)}) async-start(), calls=%async_computation.7 | async-start | bytes 1310720 | tf_op jit(solution)/shard_map/all_gather | solution.py:32
  561.9 121.7 %reduce-scatter.3.cloned.1.call-start = ((), (), s32[]{:S(2)}) async-start(), calls=%async_computation.8 | async-start | bytes 2621440 | tf_op jit(solution)/shard_map/reduce_scatter | solution.py:40
  637.0 5.8 copy-start.4
  653.9 53.9 %reduce-scatter.5.cloned.1.call-start = ((), (), s32[]{:S(2)}) async-start(), calls=%async_computation.9 | async-start | bytes 655360 | tf_op jit(solution)/shard_map/reduce_scatter | solution.py:41
Sparse Core Ops, SparseCore 0:
  563.2 27.5 all-gather.2
  654.0 29.5 reduce-scatter.2
  685.9 21.8 reduce-scatter.4
where the time goes:
time: 718 us; the launch traced here: 716 us
  waiting for transfers between devices  293 us (41%)
  local copies, waits for them, and re-layouts  161 us (22%)
  other arithmetic  112 us (16%)
  blocking collectives  96.3 us (13%)
  starting transfers between devices  22.2 us (3%)
  matrix products  16.6 us (2%)
  between operations  14.5 us (2%)
    all_to_all x1, waiting for transfers between devices, body(): lax.all_to_all(up_tp, 'fs', split_axis=2, concat_axis=1, tiled=True)  148 us
    unnamed x26, local copies, waits for them, and re-layouts  113 us
    unnamed x3, other arithmetic  96.4 us
    all_to_all x1, waiting for transfers between devices, body(): lax.all_to_all(gate_tp, 'fs', split_axis=2, concat_axis=1, tiled=True)  90.4 us
    all_to_all x1, blocking collectives, body(): lax.all_to_all(gate_cast, 'tp', split_axis=0, concat_axis=2, tiled=True)  86.2 us
    reduce_scatter x1, waiting for transfers between devices, body(): by_feature = lax.psum_scatter(term, 'tp', scatter_dimension=1, tiled=True)  29.7 us
  transfers between devices with their start and end apart: 7, of which 6 were waited for; matrix products, arithmetic and copies ran while one was open for 33% of the time, Pallas kernels for 0%

commit v1 on v0

v1 whole, which is shorter than its diff:
```python
import functools

import jax
import jax.numpy as jnp
from jax import lax
from jax.experimental import pallas as pl
from jax.experimental.pallas import tpu as pltpu
from jax.sharding import PartitionSpec as P

BF16 = jnp.bfloat16
F32 = jnp.float32
CHUNKS = 4
DOWN_CHUNKS = 4
LOADS = 4


def move_kernel(
    groups, n, gain_ref, wg_ref, wu_ref, wd_ref, og_ref, ou_ref, od_ref,
    wide, wide_d, stage, extra, relay, stage_d,
    load_sem, s1s, s1r, xs, xr, zs, zr, ys, yr, ds, dr,
):
    g, f, t = lax.axis_index("grp"), lax.axis_index("fs"), lax.axis_index("tp")
    rows = wg_ref.shape[1]
    half = rows // groups
    ch = half // CHUNKS
    hidden, width = wd_ref.shape[1:]
    dh = hidden // DOWN_CHUNKS
    weights, outs = (wg_ref, wu_ref), (og_ref, ou_ref)
    items = 2 * CHUNKS

    mate = t + 1 - 2 * lax.rem(t, 2)
    peers = (t, mate, lax.rem(t + 2, n), lax.rem(mate + 2, n))
    home = f == t

    def remote(src, dst, ssem, rsem, where):
        return pltpu.make_async_remote_copy(
            src_ref=src, dst_ref=dst, send_sem=ssem, recv_sem=rsem,
            device_id=where, device_id_type=pl.DeviceIdType.MESH,
        )

    barrier = pltpu.get_barrier_semaphore()
    for k in (1, 2, 3):
        pl.semaphore_signal(barrier, inc=1, device_id=(g, f, peers[k]), device_id_type=pl.DeviceIdType.MESH)
    for d in range(1, n):
        pl.semaphore_signal(barrier, inc=1, device_id=(g, lax.rem(f + d, n), t), device_id_type=pl.DeviceIdType.MESH)
    pl.semaphore_signal(barrier, inc=1, device_id=(1 - g, f, t), device_id_type=pl.DeviceIdType.MESH)
    pl.semaphore_wait(barrier, 2 * n - 1)

    def own_row(c):
        return pl.multiple_of(g * half + c * ch, ch)

    def other_row(c):
        return pl.multiple_of((1 - g) * half + c * ch, ch)

    def at_rows(u, source, row):
        return outs[u].at[pl.ds(pl.multiple_of(source * rows + row, ch), ch), :]

    def first(k, u, c):
        return remote(stage.at[k, u, c], relay.at[k - 1, u, c], s1s.at[k, u, c], s1r.at[k, u, c], (g, f, peers[k]))

    def first_home(k, u, c):
        return remote(stage.at[k, u, c], at_rows(u, f, own_row(c)), s1s.at[k, u, c], s1r.at[k, u, c], (g, f, peers[k]))

    def own_home(u, c):
        return pltpu.make_async_copy(stage.at[0, u, c], at_rows(u, f, own_row(c)), s1s.at[0, u, c])

    def extra_home(u, c):
        return pltpu.make_async_copy(extra.at[0, u, c], at_rows(u, f, other_row(c)), xs.at[0, u, c])

    def extra_mate(u, c):
        return remote(extra.at[1, u, c], at_rows(u, f, other_row(c)), xs.at[1, u, c], xr.at[u, c], (g, f, mate))

    def layer(k, u, c):
        src = stage.at[0, u, c] if k == 0 else relay.at[k - 1, u, c]
        return remote(src, at_rows(u, f, own_row(c)), zs.at[k, u, c], zr.at[f, u, c], (g, peers[k], t))

    def layer_in(source, u, c):
        piece = at_rows(u, source, own_row(c))
        return remote(piece, piece, zs.at[0, u, c], zr.at[source, u, c], (1 - g, f, t))

    def across(source, u, c):
        piece = at_rows(u, source, own_row(c))
        return remote(piece, piece, ys.at[source, u, c], yr.at[source, u, c], (1 - g, f, t))

    def down(k, c):
        src = stage_d.at[k, c]
        dst = od_ref.at[pl.ds(c * dh, dh), pl.ds(pl.multiple_of(t * width, 128), width)]
        if k == 0:
            return pltpu.make_async_copy(src, dst, ds.at[0, c])
        return remote(src, dst, ds.at[k, c], dr.at[k, c], (g, f, peers[k]))

    order = (2, 0, 3, 1)

    def load(u, k, row, slot):
        return pltpu.make_async_copy(weights[u].at[peers[k], pl.ds(row, ch), :], wide.at[slot], load_sem.at[slot])

    def load_d(k, c, slot):
        return pltpu.make_async_copy(wd_ref.at[peers[k], pl.ds(c * dh, dh), :], wide_d.at[slot], load_sem.at[LOADS + slot])

    def fold(slot, row, dst):
        scale = gain_ref[pl.ds(row, ch), :]
        dst[...] = (wide[slot] * scale).astype(BF16)

    for j, k in enumerate(order):
        load(0, k, own_row(0), j).start()
    for u in range(2):
        def trip(c, _, u=u):
            for j, k in enumerate(order):
                load(u, k, own_row(c), j).wait()
                fold(j, own_row(c), stage.at[k, u, c])

                @pl.when(c < CHUNKS - 1)
                def _():
                    load(u, k, own_row(c + 1), j).start()

                if u == 0:
                    @pl.when(c == CHUNKS - 1)
                    def _():
                        load(1, k, own_row(0), j).start()

                if k == 0:
                    @pl.when(home)
                    def _():
                        own_home(u, c).start()

                    @pl.when(jnp.logical_not(home))
                    def _():
                        layer(0, u, c).start()
                else:
                    @pl.when(home)
                    def _():
                        first_home(k, u, c).start()

                    @pl.when(jnp.logical_not(home))
                    def _():
                        first(k, u, c).start()
            return 0

        lax.fori_loop(0, CHUNKS, trip, 0)

    for j, k in enumerate(order):
        load_d(k, 0, j).start()

    def trip_d(c, _):
        for j, k in enumerate(order):
            load_d(k, c, j).wait()
            stage_d[k, c] = wide_d[j].astype(BF16)

            @pl.when(c < DOWN_CHUNKS - 1)
            def _():
                load_d(k, c + 1, j).start()

            down(k, c).start()
        return 0

    lax.fori_loop(0, DOWN_CHUNKS, trip_d, 0)

    @pl.when(home)
    def _():
        for u in range(2):
            def trip_x(c, _, u=u):
                for k in (0, 1):
                    copy = load(u, k, other_row(c), k)
                    copy.start()
                    copy.wait()
                    fold(k, other_row(c), extra.at[k, u, c])
                    (extra_home if k == 0 else extra_mate)(u, c).start()
                return 0

            lax.fori_loop(0, CHUNKS, trip_x, 0)

    def forward_z(k, u, c):
        away = peers[k] != f

        @pl.when(away)
        def _():
            first(k, u, c).wait_recv()
            layer(k, u, c).start()

        @pl.when(jnp.logical_not(away))
        def _():
            first_home(k, u, c).wait_recv()
            if k >= 2:
                across(f, u, c).start()

    def forward_y(d, u, c):
        for sign in (1, -1):
            source = f + sign * d

            @pl.when((source >= 0) & (source < n))
            def _():
                layer_in(source, u, c).wait_recv()
                across(source, u, c).start()

    lag = min(2, items)

    def at_item(fn, i):
        u, c = i // CHUNKS, lax.rem(i, CHUNKS)
        for v in range(2):
            @pl.when(u == v)
            def _():
                fn(v, c)

    def trip_f(i, _):
        def z_part(u, c):
            for k in (1, 2, 3):
                forward_z(k, u, c)

        at_item(z_part, i)

        @pl.when(i >= lag)
        def _():
            at_item(functools.partial(forward_y, 1), i - lag)

        return 0

    lax.fori_loop(0, items, trip_f, 0)

    def trip_t(i, _):
        at_item(functools.partial(forward_y, 1), i)
        return 0

    lax.fori_loop(items - lag, items, trip_t, 0)

    def trip_r(i, _):
        at_item(functools.partial(forward_y, 2), i)
        at_item(functools.partial(forward_y, 3), i)
        return 0

    lax.fori_loop(0, items, trip_r, 0)

    for u in range(2):
        def trip_w(c, _, u=u):
            @pl.when(home)
            def _():
                own_home(u, c).wait()
                extra_home(u, c).wait()
                extra_mate(u, c).wait_send()

            @pl.when(jnp.logical_not(home))
            def _():
                layer(0, u, c).wait_send()

            @pl.when(f == mate)
            def _():
                extra_mate(u, c).wait_recv()

            for k in (1, 2, 3):
                first(k, u, c).wait_send()

                @pl.when(peers[k] != f)
                def _():
                    layer(k, u, c).wait_send()

                if k >= 2:
                    @pl.when(peers[k] == f)
                    def _():
                        across(f, u, c).wait()

            for d in range(1, n):
                for sign in (1, -1):
                    source = f + sign * d

                    @pl.when((source >= 0) & (source < n))
                    def _():
                        across(source, u, c).wait()
            return 0

        lax.fori_loop(0, CHUNKS, trip_w, 0)

    def trip_wd(c, _):
        for k in range(n):
            down(k, c).wait()
        return 0

    lax.fori_loop(0, DOWN_CHUNKS, trip_wd, 0)


def move(groups, n, gain, w_gate, w_up, w_down):
    experts, rows, cols = w_gate.shape
    hidden, width = w_down.shape[1:]
    ch = rows // groups // CHUNKS
    dh = hidden // DOWN_CHUNKS
    dma = pltpu.SemaphoreType.DMA
    hbm = pl.BlockSpec(memory_space=pl.ANY)
    return pl.pallas_call(
        functools.partial(move_kernel, groups, n),
        out_shape=(
            jax.ShapeDtypeStruct((rows * n, cols), BF16),
            jax.ShapeDtypeStruct((rows * n, cols), BF16),
            jax.ShapeDtypeStruct((hidden, width * n), BF16),
        ),
        in_specs=[pl.BlockSpec(memory_space=pltpu.VMEM), hbm, hbm, hbm],
        out_specs=(hbm, hbm, hbm),
        scratch_shapes=[
            pltpu.VMEM((LOADS, ch, cols), F32),
            pltpu.VMEM((LOADS, dh, width), F32),
            pltpu.VMEM((n, 2, CHUNKS, ch, cols), BF16),
            pltpu.VMEM((2, 2, CHUNKS, ch, cols), BF16),
            pltpu.VMEM((n - 1, 2, CHUNKS, ch, cols), BF16),
            pltpu.VMEM((n, DOWN_CHUNKS, dh, width), BF16),
            dma((2 * LOADS,)),
            dma((n, 2, CHUNKS)),
            dma((n, 2, CHUNKS)),
            dma((2, 2, CHUNKS)),
            dma((2, CHUNKS)),
            dma((n, 2, CHUNKS)),
            dma((n, 2, CHUNKS)),
            dma((n, 2, CHUNKS)),
            dma((n, 2, CHUNKS)),
            dma((n, DOWN_CHUNKS)),
            dma((n, DOWN_CHUNKS)),
        ],
        name="move_weights",
        compiler_params=pltpu.CompilerParams(
            collective_id=0, has_side_effects=True, vmem_limit_bytes=56 << 20
        ),
    )(gain.reshape(rows, 1), w_gate, w_up, w_down)


def hand_over(mesh, gain, w_gate, w_up, w_down):
    groups, n, tp = mesh.shape["grp"], mesh.shape["fs"], mesh.shape["tp"]
    rows, cols = w_gate.shape[1:]
    hidden, width = w_down.shape[1:]
    direct = (
        groups == 2 and n == 4 and tp == 4 and w_gate.shape[0] == tp
        and cols % 128 == 0 and width % 128 == 0
        and rows % (groups * CHUNKS * 16) == 0 and hidden % (DOWN_CHUNKS * 16) == 0
    )
    if direct:
        gate, up, down = move(groups, n, gain, w_gate, w_up, w_down)
        return gate[None], up[None], down[None]
    gate = (w_gate * gain[None, :, None]).astype(BF16)
    up = (w_up * gain[None, :, None]).astype(BF16)
    spread = functools.partial(lax.all_to_all, axis_name="tp", split_axis=0, concat_axis=2, tiled=True)
    gate, up, down = spread(gate), spread(up), spread(w_down.astype(BF16))
    stack = functools.partial(lax.all_to_all, axis_name="fs", split_axis=2, concat_axis=1, tiled=True)
    return stack(gate), stack(up), down


def body(mesh, tokens, routes, route_logits, gain, w_gate, w_up, w_down):
    values = tokens.astype(F32)
    mean_square = jnp.mean(values * values, axis=-1, keepdims=True)
    normed = (values * lax.rsqrt(mean_square + 1e-06)).astype(BF16)
    expert_id = lax.axis_index("tp")
    first = jax.nn.sigmoid(route_logits[:, 0] - route_logits[:, 1])
    second = jax.nn.sigmoid(route_logits[:, 1] - route_logits[:, 0])
    weight_col = first * (routes[:, 0] == expert_id).astype(F32)
    weight_col = (weight_col + second * (routes[:, 1] == expert_id).astype(F32)).astype(BF16)
    piece_rows = lax.all_gather(normed, "fs", axis=0, tiled=True)
    piece_weight = lax.all_gather(weight_col, "fs", axis=0, tiled=True)
    gate_served, up_served, down_served = hand_over(mesh, gain, w_gate, w_up, w_down)
    gate_act = jnp.dot(piece_rows, gate_served[0], preferred_element_type=F32)
    up_act = jnp.dot(piece_rows, up_served[0], preferred_element_type=F32)
    hidden_rows = jax.nn.silu(gate_act) * up_act * piece_weight[:, None].astype(F32)
    hidden = hidden_rows.astype(BF16)
    term = jnp.dot(hidden, down_served[0], preferred_element_type=F32)
    by_feature = lax.psum_scatter(term, "tp", scatter_dimension=1, tiled=True)
    mixed = lax.psum_scatter(by_feature, "fs", scatter_dimension=0, tiled=True)
    return (gate_served, up_served, down_served, mixed.astype(BF16))


def solution(mesh):
    return jax.shard_map(
        functools.partial(body, mesh),
        mesh=mesh,
        in_specs=(
            P(("grp", "fs"), None),
            P(("grp", "fs"), None),
            P(("grp", "fs"), None),
            P("fs"),
            P(None, "fs", "tp"),
            P(None, "fs", "tp"),
            P(None, "fs", "tp"),
        ),
        out_specs=(
            P(("grp", "tp"), None, "fs"),
            P(("grp", "tp"), None, "fs"),
            P(("grp", "tp"), "fs", None),
            P(("grp", "fs"), "tp"),
        ),
        check_vma=False,
    )
```

time: 718 us -> 368 us (0.51)
  Pallas kernels: 0 us -> 164 us
  waiting for transfers between devices: 293 us -> 134 us
  local copies, waits for them, and re-layouts: 161 us -> 19.6 us
  other arithmetic: 112 us -> 5.2 us
  blocking collectives: 96.3 us -> 13.5 us
  starting transfers between devices: 22.2 us -> 0.12 us
    all_to_all x4 -> x0, waiting for transfers between devices: 250 us -> none  [the longest x1 148 us: body(): lax.all_to_all(up_tp, 'fs', split_axis=2, concat_axis=1, tiled=True)]
    pallas_call x0 -> x1, Pallas kernels: none -> 164 us  [move(): pl.pallas_call(functools.partial(move_kernel, groups, n), out_shape=(jax....]
    unnamed x3 -> x2, other arithmetic: 96.4 us -> 0.77 us
    unnamed x26 -> x12, local copies, waits for them, and re-layouts: 113 us -> 18.1 us
    all_to_all x1 -> x0, blocking collectives: 86.2 us -> none  [body(): lax.all_to_all(gate_cast, 'tp', split_axis=0, concat_axis=2, tiled=True)]
    reduce_scatter x1, waiting for transfers between devices: 29.7 us -> 110 us  [body(): by_feature = lax.psum_scatter(term, 'tp', scatter_dimension=1, tiled=True)]
    all_to_all x4 -> x0, local copies, waits for them, and re-layouts: 47.3 us -> none  [the longest x1 13.7 us: body(): lax.all_to_all(gate_cast, 'tp', split_axis=0, concat_axis=2, tiled=True)]
    all_to_all x4 -> x0, starting transfers between devices: 22 us -> none  [the longest x1 5.68 us: body(): lax.all_to_all(gate_tp, 'fs', split_axis=2, concat_axis=1, tiled=True)]
  transfers between devices with their start and end apart: 7 -> 3, of which waited for: 6 -> 2; matrix products, arithmetic and copies ran while one was open for 33% -> 1% of each run, Pallas kernels for 0% -> 45%
where the time goes in v1:
time: 368 us; the launch traced here: 367 us
  Pallas kernels  164 us (45%)
  waiting for transfers between devices  134 us (36%)
  local copies, waits for them, and re-layouts  19.6 us (5%)
  matrix products  16.7 us (5%)
  between operations  14.5 us (4%)
  blocking collectives  13.5 us (4%)
  other arithmetic  5.2 us (1%)
    pallas_call x1, Pallas kernels, move(): pl.pallas_call(functools.partial(move_kernel, groups, n), out_shape=(jax....  164 us
    reduce_scatter x1, waiting for transfers between devices, body(): by_feature = lax.psum_scatter(term, 'tp', scatter_dimension=1, tiled=True)  110 us
    reduce_scatter x1, waiting for transfers between devices, body(): mixed = lax.psum_scatter(by_feature, 'fs', scatter_dimension=0, tiled=True)  24.1 us
    unnamed x12, local copies, waits for them, and re-layouts  18.1 us
    unnamed x1, blocking collectives  13.5 us
    dot_general x1, matrix products, body(): term = jnp.dot(hidden, down_served[0], preferred_element_type=F32)  11.1 us
  transfers between devices with their start and end apart: 3, of which 2 were waited for; matrix products, arithmetic and copies ran while one was open for 1% of the time, Pallas kernels for 45%

profile of v1, /device:TPU:0, one launch (start us, length us, event | category | flops | bytes accessed | tf_op | source)
XLA Modules:
  0.0 367.1 jit_solution(3449147057436699064)
XLA Ops:
  7.2 0.0 all-gather.3.cloned.1.call-start
  7.2 1.1 fusion.3
  8.3 1.8 fusion.4
  10.1 0.0 all-gather.3.cloned.1.call-update
  10.1 0.0 reduce-scatter.3.cloned.1.call-start
  10.2 1.2 dynamic-slice
  12.1 0.8 convert_bitcast_fusion
  12.9 0.2 dynamic-update-slice
  13.1 13.5 %all-reduce = bf16[256]{0:T(256)(128)(2,1)S(1)} all-reduce(bf16[256]{0:T(256)(128)(2,1)S(1)} %dynamic-update-slice), channel_id=2, replica_groups=mesh['grp'=2,'fs'=4,'tp'=4] {'fs'}, use_global_device_ids=true, to_apply=%add | all-reduce | flops 256 | bytes 1024
  26.7 1.5 copy.11.gain_ref
  28.2 163.7 %move_weights.1 = (bf16[2048,1792]{1,0:T(8,128)(2,1)}, bf16[2048,1792]{1,0:T(8,128)(2,1)}, bf16[1792,2048]{1,0:T(8,128)(2,1)}) custom-call(f32[512,1]{1,0:T(8,128)} %copy.11.gain_ref, f32[4,512,1792]{2,1,0:T(8,128)} %wg_ref.1, f32[4,512,1792]{2,1,0:T(8,128)} %wu_ref.1, f32[4,1792,512]{2,1,0:T(8,128)} %wd_ref.1), custom_call_target="tpu_custom_call" | custom-call | tf_op jit(solution)/shard_map/move_weights/pallas_call | solution.py:286
  191.9 0.0 all-gather.3.cloned.1.call-done
  191.9 0.0 copy-start
  191.9 5.5 %fusion.7 = f32[256,1792]{1,0:T(8,128)S(1)} fusion(bf16[256,2048]{1,0:T(8,128)(2,1)} %all-gather.3.cloned.1.call-done, bf16[2048,1792]{1,0:T(8,128)(2,1)} %get-tuple-element.7), kind=kOutput, calls=%fused_computation.14 | convolution fusion | flops 1879048192 | bytes 10223616 | tf_op jit(solution)/shard_map/dot_general | solution.py:353
  197.5 0.0 copy-done
  197.5 11.1 %fusion.2 = f32[256,2048]{1,0:T(8,128)} fusion(bf16[1792,2048]{1,0:T(8,128)(2,1)} %get-tuple-element.9, bf16[256,2048]{1,0:T(8,128)(2,1)S(1)} %copy-done, bf16[2048,1792]{1,0:T(8,128)(2,1)} %get-tuple-element.8, f32[256,1792]{1,0:T(8,128)S(1)} %fusion.7, f32[256]{0:T(256)S(1)} %convert_element_type.29), kind=kOutput, calls=%fused_computation.3 | convolution fusion | flops 3761307648 | bytes 19661824 | tf_op jit(solution)/shard_map/dot_general | solution.py:357
  208.6 0.0 reduce-scatter.3.cloned.1.call-update
  208.6 0.0 reduce-scatter.5.cloned.1.call-start
  208.7 109.7 %reduce-scatter.3.cloned.1.call-done = f32[256,512]{1,0:T(8,128)} async-done(((f32[256,2048]{1,0:T(8,128)}), f32[256,512]{1,0:T(8,128)}) %reduce-scatter.3.cloned.1.call-update) | async-done | bytes 524304 | tf_op jit(solution)/shard_map/reduce_scatter | solution.py:358
  318.3 0.0 reduce-scatter.5.cloned.1.call-update
  318.3 24.1 %reduce-scatter.5.cloned.1.call-done = f32[64,512]{1,0:T(8,128)} async-done(((f32[256,512]{1,0:T(8,128)}), f32[64,512]{1,0:T(8,128)}) %reduce-scatter.5.cloned.1.call-update) | async-done | bytes 131088 | tf_op jit(solution)/shard_map/reduce_scatter | solution.py:359
  342.5 1.5 convert_element_type.26
  344.0 0.0 slice-start
  344.0 6.8 %copy.16 = bf16[1,2048,1792]{2,1,0:T(8,128)(2,1)} copy(bf16[1,2048,1792]{2,1,0:T(8,128)(2,1)} %bitcast.16) | data formatting | bytes 14680064
  350.8 0.0 slice-start.1
  350.8 6.8 %copy.17 = bf16[1,2048,1792]{2,1,0:T(8,128)(2,1)} copy(bf16[1,2048,1792]{2,1,0:T(8,128)(2,1)} %bitcast.15) | data formatting | bytes 14680064
  357.5 0.0 slice-done
  357.5 0.0 slice-done.1
  357.5 3.0 copy.18
  (4 shorter events, 0.0 us)
Async XLA Ops:
  7.2 184.7 %all-gather.3.cloned.1.call-start = ((), (), s32[]{:S(2)}) async-start(), calls=%async_computation.2 | async-start | bytes 1310720 | tf_op jit(solution)/shard_map/all_gather | solution.py:350
  10.1 308.2 %reduce-scatter.3.cloned.1.call-start = ((), (), s32[]{:S(2)}) async-start(), calls=%async_computation.3 | async-start | bytes 2621440 | tf_op jit(solution)/shard_map/reduce_scatter | solution.py:358
  191.9 5.6 %copy-start = (bf16[256,2048]{1,0:T(8,128)(2,1)S(1)}, bf16[256,2048]{1,0:T(8,128)(2,1)}, u32[]{:S(2)}) copy-start(bf16[256,2048]{1,0:T(8,128)(2,1)} %all-gather.3.cloned.1.call-done) | copy-start | bytes 3145732
  208.6 133.9 %reduce-scatter.5.cloned.1.call-start = ((), (), s32[]{:S(2)}) async-start(), calls=%async_computation.4 | async-start | bytes 655360 | tf_op jit(solution)/shard_map/reduce_scatter | solution.py:359
  344.0 13.5 %slice-start = ((s8[7340032]{0:T(1024)(128)(4,1)}), s8[4194304]{0:T(1024)(128)(4,1)S(1)}, s32[]{:S(2)}) async-start(s8[7340032]{0:T(1024)(128)(4,1)} %bitcast.12), calls=%async_computation.5 | async-start | bytes 8388608
  350.8 6.8 %slice-start.1 = ((s8[7340032]{0:T(1024)(128)(4,1)}), s8[3145728]{0:T(1024)(128)(4,1)S(1)}, s32[]{:S(2)}) async-start(s8[7340032]{0:T(1024)(128)(4,1)} %bitcast.12), calls=%async_computation.6 | async-start | bytes 6291456
Sparse Core Ops, SparseCore 0:
  10.2 79.5 all-gather.2
  208.7 109.5 reduce-scatter.2
  320.6 21.8 reduce-scatter.4

commit v2 on v1

--- a/solution.py
+++ b/solution.py
@@ -11,6 +11,7 @@
 F32 = jnp.float32
 CHUNKS = 4
 DOWN_CHUNKS = 4
+LAGS = (3, 5, 7)
 LOADS = 4
 
 
@@ -192,8 +193,6 @@
                 layer_in(source, u, c).wait_recv()
                 across(source, u, c).start()
 
-    lag = min(2, items)
-
     def at_item(fn, i):
         u, c = i // CHUNKS, lax.rem(i, CHUNKS)
         for v in range(2):
@@ -206,28 +205,20 @@
             for k in (1, 2, 3):
                 forward_z(k, u, c)
 
-        at_item(z_part, i)
-
-        @pl.when(i >= lag)
+        @pl.when(i < items)
         def _():
-            at_item(functools.partial(forward_y, 1), i - lag)
+            at_item(z_part, i)
+
+        for d in range(1, n):
+            lag = LAGS[d - 1]
+
+            @pl.when((i >= lag) & (i < items + lag))
+            def _():
+                at_item(functools.partial(forward_y, d), i - lag)
 
         return 0
 
-    lax.fori_loop(0, items, trip_f, 0)
-
-    def trip_t(i, _):
-        at_item(functools.partial(forward_y, 1), i)
-        return 0
-
-    lax.fori_loop(items - lag, items, trip_t, 0)
-
-    def trip_r(i, _):
-        at_item(functools.partial(forward_y, 2), i)
-        at_item(functools.partial(forward_y, 3), i)
-        return 0
-
-    lax.fori_loop(0, items, trip_r, 0)
+    lax.fori_loop(0, items + max(LAGS), trip_f, 0)
 
     for u in range(2):
         def trip_w(c, _, u=u):
@@ -318,24 +309,154 @@
     )(gain.reshape(rows, 1), w_gate, w_up, w_down)
 
 
-def hand_over(mesh, gain, w_gate, w_up, w_down):
+def mix_kernel(rows_ref, weight_ref, gate_ref, up_ref, down_ref, gate_out, up_out, down_out, term_ref, total):
+    j = pl.program_id(0)
+
+    @pl.when(j == 0)
+    def _():
+        total[...] = jnp.zeros_like(total)
+
+    gate, up, down = gate_ref[...], up_ref[...], down_ref[...]
+    gate_out[...], up_out[...], down_out[...] = gate, up, down
+    x = rows_ref[...]
+    gate_act = jnp.dot(x, gate, preferred_element_type=F32)
+    up_act = jnp.dot(x, up, preferred_element_type=F32)
+    scale = weight_ref[:, :1].astype(F32)
+    hidden = (gate_act / (1.0 + jnp.exp(-gate_act)) * up_act * scale).astype(BF16)
+    total[...] += jnp.dot(hidden, down, preferred_element_type=F32)
+
+    @pl.when(j == pl.num_programs(0) - 1)
+    def _():
+        term_ref[...] = total[...].astype(BF16)
+
+
+def mix(packed, depth, gate, up, down):
+    count = packed.shape[0]
+    cols = gate.shape[1]
+    wide = down.shape[1]
+    tile = next(w for w in (256, 128) if cols % w == 0)
+    whole = pl.BlockSpec((count, depth), lambda j: (0, 0))
+    column = pl.BlockSpec((depth, tile), lambda j: (0, j))
+    row = pl.BlockSpec((tile, wide), lambda j: (j, 0))
+    return pl.pallas_call(
+        mix_kernel,
+        grid=(cols // tile,),
+        out_shape=(
+            jax.ShapeDtypeStruct(gate.shape, BF16),
+            jax.ShapeDtypeStruct(up.shape, BF16),
+            jax.ShapeDtypeStruct(down.shape, BF16),
+            jax.ShapeDtypeStruct((count, wide), BF16),
+        ),
+        in_specs=[whole, pl.BlockSpec((count, 128), lambda j: (0, depth // 128)), column, column, row],
+        out_specs=(column, column, row, pl.BlockSpec((count, wide), lambda j: (0, 0))),
+        scratch_shapes=[pltpu.VMEM((count, wide), F32)],
+        name="mix_tokens",
+        compiler_params=pltpu.CompilerParams(vmem_limit_bytes=48 << 20),
+    )(packed, packed, gate, up, down)
+
+
+def sum_kernel(n, term_ref, out_ref, near, near_in, far, far_in, last, last_in, s1, r1, s2, r2, s3, r3):
+    g, f, t = lax.axis_index("grp"), lax.axis_index("fs"), lax.axis_index("tp")
+    mesh_id = pl.DeviceIdType.MESH
+    width = out_ref.shape[1]
+    count = out_ref.shape[0]
+    mate = t + 1 - 2 * lax.rem(t, 2)
+    over = lax.rem(t + 2, n)
+    mate_over = lax.rem(mate + 2, n)
+
+    barrier = pltpu.get_barrier_semaphore()
+    for e in (mate, over):
+        pl.semaphore_signal(barrier, inc=1, device_id=(g, f, e), device_id_type=mesh_id)
+    for d in range(1, n):
+        pl.semaphore_signal(barrier, inc=1, device_id=(g, lax.rem(f + d, n), t), device_id_type=mesh_id)
+    pl.semaphore_wait(barrier, n + 1)
+
+    def block(layer, column):
+        return term_ref.at[pl.ds(pl.multiple_of(layer * count, count), count), pl.ds(pl.multiple_of(column * width, width), width)]
+
+    def remote(src, dst, ssem, rsem, where):
+        return pltpu.make_async_remote_copy(
+            src_ref=src, dst_ref=dst, send_sem=ssem, recv_sem=rsem, device_id=where, device_id_type=mesh_id
+        )
+
+    layers = [lax.rem(f + d, n) for d in (2, 1, 3, 0)]
+
+    def to_mate(i, h):
+        column = mate_over if h == 0 else mate
+        return remote(block(layers[i], column), near_in.at[h, i], s1.at[h, i], r1.at[h, i], (g, f, mate))
+
+    def to_over(i):
+        return remote(far.at[i], far_in.at[i], s2.at[i], r2.at[i], (g, f, over))
+
+    def to_layer(i):
+        return remote(last.at[i], last_in.at[f], s3.at[i], r3.at[f], (g, layers[i], t))
+
+    def from_layer(layer):
+        return remote(last.at[0], last_in.at[layer], s3.at[0], r3.at[layer], (g, layer, t))
+
+    for i in range(n):
+        for h in range(2):
+            to_mate(i, h).start()
+    for i in range(n):
+        to_mate(i, 0).wait_recv()
+        far[i] = (block(layers[i], over)[...].astype(F32) + near_in[0, i].astype(F32)).astype(BF16)
+        to_mate(i, 1).wait_recv()
+        near[i] = block(layers[i], t)[...].astype(F32) + near_in[1, i].astype(F32)
+        to_over(i).start()
+    for i in range(n):
+        to_over(i).wait_recv()
+        near[i] = near[i] + far_in[i].astype(F32)
+        if i < n - 1:
+            last[i] = near[i].astype(BF16)
+            to_layer(i).start()
+    total = near[n - 1]
+    for d in range(1, n):
+        layer = lax.rem(f + d, n)
+        from_layer(layer).wait_recv()
+        total = total + last_in[layer].astype(F32)
+    out_ref[...] = total.astype(BF16)
+    for i in range(n):
+        for h in range(2):
+            to_mate(i, h).wait_send()
+        to_over(i).wait_send()
+        if i < n - 1:
+            to_layer(i).wait_send()
+
+
+def sum_terms(n, term):
+    count, width = term.shape[0] // n, term.shape[1] // n
+    dma = pltpu.SemaphoreType.DMA
+    vmem = pl.BlockSpec(memory_space=pltpu.VMEM)
+    piece = (count, width)
+    return pl.pallas_call(
+        functools.partial(sum_kernel, n),
+        out_shape=jax.ShapeDtypeStruct(piece, BF16),
+        in_specs=[vmem],
+        out_specs=vmem,
+        scratch_shapes=[
+            pltpu.VMEM((n, *piece), F32),
+            pltpu.VMEM((2, n, *piece), BF16),
+            pltpu.VMEM((n, *piece), BF16),
+            pltpu.VMEM((n, *piece), BF16),
+            pltpu.VMEM((n, *piece), BF16),
+            pltpu.VMEM((n, *piece), BF16),
+            dma((2, n)), dma((2, n)), dma((n,)), dma((n,)), dma((n,)), dma((n,)),
+        ],
+        name="sum_terms",
+        compiler_params=pltpu.CompilerParams(collective_id=1, has_side_effects=True),
+    )(term)
+
+
+def fits(mesh, tokens, w_gate, w_down):
     groups, n, tp = mesh.shape["grp"], mesh.shape["fs"], mesh.shape["tp"]
     rows, cols = w_gate.shape[1:]
     hidden, width = w_down.shape[1:]
-    direct = (
+    return (
         groups == 2 and n == 4 and tp == 4 and w_gate.shape[0] == tp
-        and cols % 128 == 0 and width % 128 == 0
+        and cols == hidden and cols % 128 == 0 and width % 128 == 0 and tokens.shape[0] % 16 == 0
         and rows % (groups * CHUNKS * 16) == 0 and hidden % (DOWN_CHUNKS * 16) == 0
+        and tokens.shape[0] * n <= 512
     )
-    if direct:
-        gate, up, down = move(groups, n, gain, w_gate, w_up, w_down)
-        return gate[None], up[None], down[None]
-    gate = (w_gate * gain[None, :, None]).astype(BF16)
-    up = (w_up * gain[None, :, None]).astype(BF16)
-    spread = functools.partial(lax.all_to_all, axis_name="tp", split_axis=0, concat_axis=2, tiled=True)
-    gate, up, down = spread(gate), spread(up), spread(w_down.astype(BF16))
-    stack = functools.partial(lax.all_to_all, axis_name="fs", split_axis=2, concat_axis=1, tiled=True)
-    return stack(gate), stack(up), down
 
 
 def body(mesh, tokens, routes, route_logits, gain, w_gate, w_up, w_down):
@@ -347,17 +468,27 @@
     second = jax.nn.sigmoid(route_logits[:, 1] - route_logits[:, 0])
     weight_col = first * (routes[:, 0] == expert_id).astype(F32)
     weight_col = (weight_col + second * (routes[:, 1] == expert_id).astype(F32)).astype(BF16)
-    piece_rows = lax.all_gather(normed, "fs", axis=0, tiled=True)
-    piece_weight = lax.all_gather(weight_col, "fs", axis=0, tiled=True)
-    gate_served, up_served, down_served = hand_over(mesh, gain, w_gate, w_up, w_down)
-    gate_act = jnp.dot(piece_rows, gate_served[0], preferred_element_type=F32)
-    up_act = jnp.dot(piece_rows, up_served[0], preferred_element_type=F32)
-    hidden_rows = jax.nn.silu(gate_act) * up_act * piece_weight[:, None].astype(F32)
-    hidden = hidden_rows.astype(BF16)
-    term = jnp.dot(hidden, down_served[0], preferred_element_type=F32)
+    packed = jnp.concatenate([normed, jnp.broadcast_to(weight_col[:, None], (normed.shape[0], 128))], axis=1)
+    packed = lax.all_gather(packed, "fs", axis=0, tiled=True)
+    n, depth = mesh.shape["fs"], normed.shape[1]
+    if fits(mesh, tokens, w_gate, w_down):
+        gate, up, down = move(mesh.shape["grp"], n, gain, w_gate, w_up, w_down)
+        gate, up, down, term = mix(packed, depth, gate, up, down)
+        return gate[None], up[None], down[None], sum_terms(n, term)
+    gate = (w_gate * gain[None, :, None]).astype(BF16)
+    up = (w_up * gain[None, :, None]).astype(BF16)
+    spread = functools.partial(lax.all_to_all, axis_name="tp", split_axis=0, concat_axis=2, tiled=True)
+    gate, up, down = spread(gate), spread(up), spread(w_down.astype(BF16))
+    stack = functools.partial(lax.all_to_all, axis_name="fs", split_axis=2, concat_axis=1, tiled=True)
+    gate, up = stack(gate), stack(up)
+    rows, weight = packed[:, :depth], packed[:, depth : depth + 1]
+    gate_act = jnp.dot(rows, gate[0], preferred_element_type=F32)
+    up_act = jnp.dot(rows, up[0], preferred_element_type=F32)
+    hidden = (jax.nn.silu(gate_act) * up_act * weight.astype(F32)).astype(BF16)
+    term = jnp.dot(hidden, down[0], preferred_element_type=F32)
     by_feature = lax.psum_scatter(term, "tp", scatter_dimension=1, tiled=True)
     mixed = lax.psum_scatter(by_feature, "fs", scatter_dimension=0, tiled=True)
-    return (gate_served, up_served, down_served, mixed.astype(BF16))
+    return gate, up, down, mixed.astype(BF16)
 
 
 def solution(mesh):

time: 368 us -> 289 us (0.79)
  waiting for transfers between devices: 134 us -> 0.04 us
  Pallas kernels: 164 us -> 264 us
  matrix products: 16.7 us -> 0 us
  local copies, waits for them, and re-layouts: 19.6 us -> 5.29 us
  blocking collectives: 13.5 us -> 0 us
    reduce_scatter x2 -> x0, waiting for transfers between devices: 134 us -> none  [the longest x1 110 us: body(): by_feature = lax.psum_scatter(term, 'tp', scatter_dimension=1, tiled=True)]
    pallas_call x0 -> x2, Pallas kernels: none -> 96.4 us  [the longest x1 75.8 us: sum_terms(): pl.pallas_call(functools.partial(sum_kernel, n), out_shape=jax.ShapeDtype...]
    dot_general x2 -> x0, matrix products: 16.7 us -> none  [the longest x1 11.1 us: body(): term = jnp.dot(hidden, down_served[0], preferred_element_type=F32)]
    unnamed x12 -> x5, local copies, waits for them, and re-layouts: 18.1 us -> 3.68 us
    unnamed x1 -> x0, blocking collectives: 13.5 us -> none
    pallas_call x1, Pallas kernels: 164 us -> 168 us  [move(): pl.pallas_call(functools.partial(move_kernel, groups, n), out_shape=(jax....]
  transfers between devices with their start and end apart: 3 -> 1, of which waited for: 2 -> 0; matrix products, arithmetic and copies ran while one was open for 1% -> 1% of each run, Pallas kernels for 45% -> 58%
where the time goes in v2:
time: 289 us; the launch traced here: 287 us
  Pallas kernels  264 us (91%)
  between operations  14.1 us (5%)
  local copies, waits for them, and re-layouts  5.29 us (2%)
  other arithmetic  3.7 us (1%)
    pallas_call x1, Pallas kernels, move(): pl.pallas_call(functools.partial(move_kernel, groups, n), out_shape=(jax....  168 us
    pallas_call x1, Pallas kernels, sum_terms(): pl.pallas_call(functools.partial(sum_kernel, n), out_shape=jax.ShapeDtype...  75.8 us
    pallas_call x1, Pallas kernels, mix(): pl.pallas_call(mix_kernel, grid=(cols // tile,), out_shape=(jax.ShapeDtyp...  20.5 us
  transfers between devices with their start and end apart: 1, of which 0 were waited for; matrix products, arithmetic and copies ran while one was open for 1% of the time, Pallas kernels for 58%

profile of v2, /device:TPU:0, one launch (start us, length us, event | category | flops | bytes accessed | tf_op | source)
XLA Modules:
  0.0 287.5 jit_solution(16594385654594316344)
XLA Ops:
  7.2 0.0 all-gather.2.cloned.1.call-start
  7.2 1.1 fusion
  8.3 1.1 fusion.1
  9.4 0.8 convert_bitcast_fusion
  10.2 0.1 broadcast_in_dim.19
  10.3 0.7 pad_maximum_fusion
  11.0 0.0 all-gather.2.cloned.1.call-update
  11.0 1.5 copy.11.gain_ref
  12.6 168.0 %move_weights.1 = (bf16[2048,1792]{1,0:T(8,128)(2,1)}, bf16[2048,1792]{1,0:T(8,128)(2,1)}, bf16[1792,2048]{1,0:T(8,128)(2,1)}) custom-call(f32[512,1]{1,0:T(8,128)} %copy.11.gain_ref, f32[4,512,1792]{2,1,0:T(8,128)} %wg_ref.1, f32[4,512,1792]{2,1,0:T(8,128)} %wu_ref.1, f32[4,1792,512]{2,1,0:T(8,128)} %wd_ref.1), custom_call_target="tpu_custom_call" | custom-call | tf_op jit(solution)/shard_map/move_weights/pallas_call | solution.py:277
  180.6 0.0 all-gather.2.cloned.1.call-done.rows_ref.weight_ref
  180.6 0.0 copy-start
  180.6 1.2 copy-done
  181.8 20.5 %mix_tokens.1 = (bf16[2048,1792]{1,0:T(8,128)(2,1)}, bf16[2048,1792]{1,0:T(8,128)(2,1)}, bf16[1792,2048]{1,0:T(8,128)(2,1)}, bf16[256,2048]{1,0:T(8,128)(2,1)S(1)}) custom-call(bf16[256,2176]{1,0:T(8,128)(2,1)S(1)} %copy-done, bf16[256,2176]{1,0:T(8,128)(2,1)S(1)} %copy-done, bf16[2048,1792]{1,0:T(8,128)(2,1)} %get-tuple-element.11.gate_ref, ...), custom_call_target="tpu_custom_call" | custom-call | tf_op jit(solution)/shard_map/mix_tokens/pallas_call | solution.py:341
  202.4 0.0 copy-start.1
  202.4 1.0 copy-done.1
  203.3 75.8 %sum_terms.1 = bf16[64,512]{1,0:T(8,128)(2,1)} custom-call(bf16[256,2048]{1,0:T(8,128)(2,1)} %copy-done.1), custom_call_target="tpu_custom_call" | custom-call | tf_op jit(solution)/shard_map/sum_terms/pallas_call | solution.py:431
  279.2 1.5 copy.13
  (1 shorter events, 0.0 us)
Async XLA Ops:
  7.2 173.4 %all-gather.2.cloned.1.call-start = ((), (), s32[]{:S(2)}) async-start(), calls=%async_computation | async-start | bytes 1392640 | tf_op jit(solution)/shard_map/all_gather | solution.py:472
  180.6 1.2 copy-start
  202.4 1.0 copy-start.1
Sparse Core Ops, SparseCore 0:
  11.1 87.5 all-gather.1

commit v3 on v2

--- a/solution.py
+++ b/solution.py
@@ -11,7 +11,7 @@
 F32 = jnp.float32
 CHUNKS = 4
 DOWN_CHUNKS = 4
-LAGS = (3, 5, 7)
+LAGS = (2, 3, 4)
 LOADS = 4
 
 

time: 289 us -> 281 us (0.972)
  Pallas kernels: 264 us -> 256 us
    pallas_call x1, Pallas kernels: 75.8 us -> 68.4 us  [sum_terms(): pl.pallas_call(functools.partial(sum_kernel, n), out_shape=jax.ShapeDtype...]
  transfers between devices with their start and end apart: 1 -> 1, of which waited for: 0 -> 0; matrix products, arithmetic and copies ran while one was open for 1% -> 1% of each run, Pallas kernels for 58% -> 60%
where the time goes in v3:
time: 281 us; the launch traced here: 280 us
  Pallas kernels  256 us (91%)
  between operations  14.1 us (5%)
  local copies, waits for them, and re-layouts  5.29 us (2%)
  other arithmetic  3.7 us (1%)
    pallas_call x1, Pallas kernels, move(): pl.pallas_call(functools.partial(move_kernel, groups, n), out_shape=(jax....  168 us
    pallas_call x1, Pallas kernels, sum_terms(): pl.pallas_call(functools.partial(sum_kernel, n), out_shape=jax.ShapeDtype...  68.4 us
    pallas_call x1, Pallas kernels, mix(): pl.pallas_call(mix_kernel, grid=(cols // tile,), out_shape=(jax.ShapeDtyp...  20.5 us
  transfers between devices with their start and end apart: 1, of which 0 were waited for; matrix products, arithmetic and copies ran while one was open for 1% of the time, Pallas kernels for 60%

profile of v3, /device:TPU:0, one launch (start us, length us, event | category | flops | bytes accessed | tf_op | source)
XLA Modules:
  0.0 279.6 jit_solution(4929194741640382689)
XLA Ops:
  7.2 0.0 all-gather.2.cloned.1.call-start
  7.2 1.1 fusion
  8.3 1.1 fusion.1
  9.4 0.8 convert_bitcast_fusion
  10.2 0.1 broadcast_in_dim.19
  10.3 0.7 pad_maximum_fusion
  11.0 0.0 all-gather.2.cloned.1.call-update
  11.0 1.5 copy.11.gain_ref
  12.6 167.6 %move_weights.1 = (bf16[2048,1792]{1,0:T(8,128)(2,1)}, bf16[2048,1792]{1,0:T(8,128)(2,1)}, bf16[1792,2048]{1,0:T(8,128)(2,1)}) custom-call(f32[512,1]{1,0:T(8,128)} %copy.11.gain_ref, f32[4,512,1792]{2,1,0:T(8,128)} %wg_ref.1, f32[4,512,1792]{2,1,0:T(8,128)} %wu_ref.1, f32[4,1792,512]{2,1,0:T(8,128)} %wd_ref.1), custom_call_target="tpu_custom_call" | custom-call | tf_op jit(solution)/shard_map/move_weights/pallas_call | solution.py:277
  180.2 0.0 all-gather.2.cloned.1.call-done.rows_ref.weight_ref
  180.2 0.0 copy-start
  180.2 1.2 copy-done
  181.4 20.5 %mix_tokens.1 = (bf16[2048,1792]{1,0:T(8,128)(2,1)}, bf16[2048,1792]{1,0:T(8,128)(2,1)}, bf16[1792,2048]{1,0:T(8,128)(2,1)}, bf16[256,2048]{1,0:T(8,128)(2,1)S(1)}) custom-call(bf16[256,2176]{1,0:T(8,128)(2,1)S(1)} %copy-done, bf16[256,2176]{1,0:T(8,128)(2,1)S(1)} %copy-done, bf16[2048,1792]{1,0:T(8,128)(2,1)} %get-tuple-element.11.gate_ref, ...), custom_call_target="tpu_custom_call" | custom-call | tf_op jit(solution)/shard_map/mix_tokens/pallas_call | solution.py:341
  201.9 0.0 copy-start.1
  201.9 1.0 copy-done.1
  202.9 68.4 %sum_terms.1 = bf16[64,512]{1,0:T(8,128)(2,1)} custom-call(bf16[256,2048]{1,0:T(8,128)(2,1)} %copy-done.1), custom_call_target="tpu_custom_call" | custom-call | tf_op jit(solution)/shard_map/sum_terms/pallas_call | solution.py:431
  271.3 1.5 copy.13
  (1 shorter events, 0.0 us)
Async XLA Ops:
  7.2 173.0 %all-gather.2.cloned.1.call-start = ((), (), s32[]{:S(2)}) async-start(), calls=%async_computation | async-start | bytes 1392640 | tf_op jit(solution)/shard_map/all_gather | solution.py:472
  180.2 1.2 copy-start
  201.9 1.0 copy-start.1
Sparse Core Ops, SparseCore 0:
  11.1 87.5 all-gather.1
